TPU v7x, 512 devices: a whole 4x4x16 slice. The times are simulated.
512 devices in a mesh: sp: 128 (over z, x, core), tp: 4 (over y).
Axes of the slice: x: 4, y: 4, z: 16, core: 2. Of those that a mesh axis runs over, the one named last changes fastest.
Arguments:
- rows_in: bfloat16 [16384, 2048], P(('sp', 'tp')), may hold values from -8 to 8
- in_gain: float32 [2048], replicated, may hold values from 0.1 to 1.9
- query_down: bfloat16 [2048, 256], replicated, may hold values from -0.125 to 0.125
- query_gain: float32 [256], replicated, may hold values from 0.1 to 1.9
- kv_down: bfloat16 [2048, 128], replicated, may hold values from -0.125 to 0.125
- kv_gain: float32 [128], replicated, may hold values from 0.1 to 1.9
- rope_down: bfloat16 [2048, 64], replicated, may hold values from -0.125 to 0.125
- query_nope_up: bfloat16 [256, 512], P(None, 'tp'), may hold values from -0.375 to 0.375
- query_rope_up: bfloat16 [256, 256], P(None, 'tp'), may hold values from -0.375 to 0.375
- key_up: bfloat16 [128, 512], P(None, 'tp'), may hold values from -2.9811459 to 2.9811459
- value_up: bfloat16 [128, 512], P(None, 'tp'), may hold values from -0.5 to 0.5
- rec_query: bfloat16 [2048, 256], P(None, 'tp'), may hold values from -0.125 to 0.125
- rec_key: bfloat16 [2048, 256], P(None, 'tp'), may hold values from -0.125 to 0.125
- rec_value: bfloat16 [2048, 512], P(None, 'tp'), may hold values from -0.125 to 0.125
- gate_weight: bfloat16 [2048, 4, 4], P(None, None, 'tp'), may hold values from -0.125 to 0.125
- forget_level: float32 [16384, 2, 4], P('sp', None, 'tp'), may hold values from 0 to 14
- head_gain: float32 [512], P('tp'), may hold values from 0.1 to 1.9
- init_state: float32 [2, 4, 64, 128], P(None, 'tp'), may hold values from -384 to 384
- init_norm: float32 [2, 4, 64], P(None, 'tp'), may hold values from -384 to 384
- out_attn: bfloat16 [512, 2048], P('tp'), may hold values from -0.25 to 0.25
- out_rec: bfloat16 [512, 2048], P('tp'), may hold values from -0.25 to 0.25
Outputs:
- mixed_out: bfloat16 [16384, 2048], P(('sp', 'tp'))
All inputs are finite; a program needn't handle non-finite values.
Results may differ from a plain program's by a relative error of at most 0.023.
Values may be sent and summed in bfloat16 or wider, within the bound.
A program may use at most 64 MiB of HBM per device.

v0:
```python
import math

import jax
import jax.numpy as jnp
from jax import lax
from jax.sharding import Mesh
from jax.sharding import PartitionSpec as P

NOPE = 128
ROPE = 64
VH = 128
MK = 64
MV = 128
MBLOCK = 128
SP = ("sp_0", "sp_1", "sp_2")
SP_TP = ("sp_0", "sp_1", "sp_2", "tp")


EPS = 1e-06
NEG = -1e30
HIGHEST = lax.Precision.HIGHEST


def joined_along(blocks, dim):
    blocks = jnp.moveaxis(blocks, 0, dim)
    shape = blocks.shape
    return blocks.reshape(*shape[:dim], shape[dim] * shape[dim + 1], *shape[dim + 2 :])


def from_everyone(x, axis):
    copies = jnp.broadcast_to(x, (lax.axis_size(axis), *x.shape))
    return lax.all_to_all(copies, axis, split_axis=0, concat_axis=0, tiled=True)


def collect(x, axis, dim):
    return joined_along(from_everyone(x, axis), dim)


def sent_together(arrays, axis, dim, along):
    both = jnp.concatenate(arrays, axis=along)
    filled, at, finished = (lax.all_gather(both, axis, axis=dim, tiled=True), 0, [])
    for a in arrays:
        finished.append(lax.slice_in_dim(filled, at, at + a.shape[along], axis=along))
        at += a.shape[along]
    return tuple(finished)


def nothing_yet(x, identity):
    return jax.tree.map(
        lambda a, e: jnp.broadcast_to(jnp.asarray(e, a.dtype), a.shape), x, identity
    )


def collected_together(x, axis):
    leaves = jax.tree.leaves(x)
    turns = sorted(range(len(leaves)), key=lambda k: -leaves[k].size)
    width = (1, *leaves[turns[0]].shape)[-1]
    lines = [
        jnp.pad(leaves[k].reshape(-1), (0, -leaves[k].size % width)).reshape(-1, width)
        for k in turns
    ]
    both, at, found = (lax.all_gather(jnp.concatenate(lines), axis), 0, {})
    for k, line in zip(turns, lines):
        section = both[:, at : at + len(line)].reshape(len(both), -1)
        found[k] = section[:, : leaves[k].size].reshape(-1, *leaves[k].shape)
        at += len(line)
    numbers = iter(range(len(leaves)))
    return jax.tree.map(lambda _: found[next(numbers)], x)


def carried_in(x, axes, combine, identity, reverse):
    before = start = nothing_yet(x, identity)
    total = x
    for axis in reversed(axes):
        peers, mine = (lax.axis_size(axis), lax.axis_index(axis))
        pieces = collected_together(total, axis)
        inside, total = (start, start)
        for k in reversed(range(peers)) if reverse else range(peers):
            passed = k > mine if reverse else k < mine
            total = combine(total, jax.tree.map(lambda part: part[k], pieces))
            inside = jax.tree.map(lambda new, old: jnp.where(passed, new, old), total, inside)
        before = combine(inside, before)
    return before


def in_blocks(x, dim, peers):
    before, after = (x.shape[:dim], x.shape[dim + 1 :])
    return jnp.moveaxis(x.reshape(*before, peers, -1, *after), dim, 0)


def summed_on_arrival(x, axis, dim):
    blocks = in_blocks(x, dim, lax.axis_size(axis))
    arrived = lax.all_to_all(blocks, axis, split_axis=0, concat_axis=0, tiled=True)
    return arrived.astype(jnp.float32).sum(axis=0)


def rms_rows(values, gains):
    return values * lax.rsqrt(jnp.mean(values * values, axis=-1, keepdims=True) + EPS) * gains


def rotate(values, positions):
    half_len = values.shape[-1] // 2
    frequency = 10000.0 ** (-jnp.arange(half_len, dtype=jnp.float32) / half_len)
    angles = positions.astype(jnp.float32)[:, None] * frequency[None, :]
    angles = jnp.concatenate([angles, angles], axis=-1)[:, None, :]
    turned = jnp.concatenate([-values[..., half_len:], values[..., :half_len]], axis=-1)
    return values * jnp.cos(angles) + turned * jnp.sin(angles)


def recurrence(query, keys_in, value_in, log_in, log_keep, c_start, n_start, m_start, floor_value):
    head_count, seq_len = log_in.shape
    block_count = seq_len // MBLOCK
    lower_mask = jnp.tril(jnp.ones((MBLOCK, MBLOCK), bool))

    def to_blocks(array):
        return jnp.moveaxis(
            array.reshape((head_count, block_count, MBLOCK) + array.shape[2:]), 1, 0
        )

    def one_step(carried, inputs):
        c_state, n_state, m_state = carried
        q_block, k_block, v_block, in_block, keep_block = inputs
        log_cum = jnp.cumsum(keep_block, axis=-1)
        log_decay = jnp.where(
            lower_mask, log_cum[:, :, None] - log_cum[:, None, :] + in_block[:, None, :], NEG
        )
        carry_log = log_cum + m_state[:, None]
        row_max = jnp.maximum(jnp.max(log_decay, axis=-1), carry_log)
        gated = jnp.einsum("htd,hsd->hts", q_block, k_block, precision=HIGHEST) * jnp.exp(
            log_decay - row_max[..., None]
        )
        carry_weight = jnp.exp(carry_log - row_max)
        numerator = jnp.einsum("hts,hse->hte", gated, v_block, precision=HIGHEST) + carry_weight[
            ..., None
        ] * jnp.einsum("htd,hde->hte", q_block, c_state, precision=HIGHEST)
        denominator = jnp.sum(gated, axis=-1) + carry_weight * jnp.einsum(
            "htd,hd->ht", q_block, n_state, precision=HIGHEST
        )
        result = (
            numerator
            / jnp.maximum(jnp.abs(denominator), floor_value * jnp.exp(-row_max))[..., None]
        )
        cum_end = log_cum[:, -1]
        weight_log = cum_end[:, None] - log_cum + in_block
        new_max = jnp.maximum(cum_end + m_state, jnp.max(weight_log, axis=-1))
        decay_all = jnp.exp(cum_end + m_state - new_max)
        in_weights = jnp.exp(weight_log - new_max[:, None])
        c_state = decay_all[:, None, None] * c_state + jnp.einsum(
            "hsd,hse->hde", k_block * in_weights[..., None], v_block, precision=HIGHEST
        )
        n_state = decay_all[:, None] * n_state + jnp.einsum(
            "hs,hsd->hd", in_weights, k_block, precision=HIGHEST
        )
        return ((c_state, n_state, new_max), result)

    inputs = tuple((to_blocks(array) for array in (query, keys_in, value_in, log_in, log_keep)))
    _, outputs = lax.scan(one_step, (c_start, n_start, m_start), inputs)
    return jnp.moveaxis(outputs, 0, 1).reshape(head_count, seq_len, -1)


def summary(keys_in, value_in, log_in, log_keep):
    log_cum = jnp.cumsum(log_keep, axis=-1)
    cum_end = log_cum[:, -1]
    weight_log = cum_end[:, None] - log_cum + log_in
    row_peak = jnp.max(weight_log, axis=-1)
    in_weights = jnp.exp(weight_log - row_peak[:, None])
    c_part = jnp.einsum(
        "hsd,hse->hde", keys_in * in_weights[..., None], value_in, precision=HIGHEST
    )
    n_part = jnp.einsum("hs,hsd->hd", in_weights, keys_in, precision=HIGHEST)
    return (c_part, n_part, row_peak, cum_end)


def combine(early_part, late_part):
    c_early, n_early, m_early, f_early = early_part
    c_late, n_late, m_late, f_late = late_part
    new_peak = jnp.maximum(f_late + m_early, m_late)
    carried = jnp.exp(f_late + m_early - new_peak)
    fresh = jnp.exp(m_late - new_peak)
    return (
        carried[:, None, None] * c_early + fresh[:, None, None] * c_late,
        carried[:, None] * n_early + fresh[:, None] * n_late,
        new_peak,
        f_early + f_late,
    )


def heads_first(product, head_width):
    rounded = lax.optimization_barrier(product.astype(jnp.bfloat16))
    return rounded.astype(jnp.float32).reshape(product.shape[0], -1, head_width).transpose(1, 0, 2)


def shards(
    rows_in,
    in_gain,
    query_down,
    query_gain,
    kv_down,
    kv_gain,
    rope_down,
    query_nope_up,
    query_rope_up,
    key_up,
    value_up,
    rec_query,
    rec_key,
    rec_value,
    gate_weight,
    forget_level,
    head_gain,
    init_state,
    init_norm,
    out_attn,
    out_rec,
):
    f32 = jnp.float32
    bf16 = jnp.bfloat16
    seq_rows = forget_level.shape[0]
    model_width = rows_in.shape[1]
    latent_kv = kv_down.shape[1]
    rope_width = rope_down.shape[1]
    attn_heads = value_up.shape[1] // VH
    rec_heads = head_gain.shape[0] // MV
    floor_value = float(seq_rows * lax.axis_size(SP)) ** 0.5
    normed = rms_rows(rows_in.astype(f32), in_gain).astype(bf16)
    gates_flat = gate_weight.reshape(model_width, 4 * rec_heads)
    projections = (query_down, kv_down, rope_down, rec_query, rec_key, rec_value, gates_flat)

    def project(row_piece):
        return jnp.concatenate(
            [jnp.dot(row_piece, weight, preferred_element_type=f32) for weight in projections],
            axis=1,
        )

    projected = project(collect(normed, "tp", 0))
    splits = []
    offset = 0
    for weight in projections:
        splits.append(projected[:, offset : offset + weight.shape[1]])
        offset = offset + weight.shape[1]
    positions = lax.axis_index(SP) * seq_rows + jnp.arange(seq_rows, dtype=jnp.int32)
    q_latent = rms_rows(splits[0], query_gain).astype(bf16)
    kv_latent = rms_rows(splits[1], kv_gain).astype(bf16)
    key_rope = rotate(splits[2][:, None, :], positions)[:, 0, :].astype(bf16)
    query_nope = (
        jnp.dot(q_latent, query_nope_up, preferred_element_type=f32)
        .astype(bf16)
        .reshape(seq_rows, attn_heads, NOPE)
    )
    query_rope = rotate(
        jnp.dot(q_latent, query_rope_up, preferred_element_type=f32).reshape(
            seq_rows, attn_heads, ROPE
        ),
        positions,
    ).astype(bf16)
    query_abs = jnp.einsum(
        "thn,khn->thk",
        query_nope,
        key_up.reshape(latent_kv, attn_heads, NOPE),
        preferred_element_type=f32,
    ).astype(bf16)
    abs_rows = query_abs.reshape(seq_rows * attn_heads, latent_kv)
    rope_rows = query_rope.reshape(seq_rows * attn_heads, rope_width)
    score_scale = (NOPE + ROPE) ** (-0.5)
    query_count = seq_rows * attn_heads
    start_state = (
        jnp.full((query_count,), NEG, f32),
        jnp.zeros((query_count,), f32),
        jnp.zeros((query_count, latent_kv), f32),
    )
    contract = (((1,), (1,)), ((), ()))
    carried = start_state
    key_lat, key_rot = sent_together((kv_latent, key_rope), SP, 0, 1)
    total_rows = key_lat.shape[0]
    step_rows = math.gcd(total_rows, 2048)

    def one_block(running, key_block):
        row_peak, row_mass, row_accum = running
        lat_block, rot_block = key_block
        scores = lax.dot_general(abs_rows, lat_block, contract, preferred_element_type=f32)
        scores = (
            scores + lax.dot_general(rope_rows, rot_block, contract, preferred_element_type=f32)
        ) * score_scale
        new_peak = jnp.maximum(row_peak, jnp.max(scores, axis=1))
        expo_all = jnp.exp(scores - new_peak[:, None])
        shrink = jnp.exp(row_peak - new_peak)
        row_mass = row_mass * shrink + jnp.sum(expo_all, axis=1)
        row_accum = row_accum * shrink[:, None] + jnp.dot(
            expo_all.astype(bf16), lat_block, preferred_element_type=f32
        )
        return ((new_peak, row_mass, row_accum), None)

    key_blocks = (
        key_lat.reshape(total_rows // step_rows, step_rows, latent_kv),
        key_rot.reshape(total_rows // step_rows, step_rows, rope_width),
    )
    carried, _ = lax.scan(one_block, carried, key_blocks)
    row_peak, row_mass, row_accum = carried
    attended = (row_accum / row_mass[:, None]).astype(bf16).reshape(seq_rows, attn_heads, latent_kv)
    attention_out = (
        jnp.einsum(
            "thk,khv->thv",
            attended,
            value_up.reshape(latent_kv, attn_heads, VH),
            preferred_element_type=f32,
        )
        .astype(bf16)
        .reshape(seq_rows, attn_heads * VH)
    )
    rec_q = heads_first(splits[3], MK)
    rec_k = heads_first(splits[4], MK) * MK ** (-0.5)
    rec_v = heads_first(splits[5], MV)
    gate_pre = splits[6].reshape(seq_rows, 4, rec_heads)
    input_fwd = gate_pre[:, 0].T
    keep_fwd = jax.nn.log_sigmoid(gate_pre[:, 1] + forget_level[:, 0]).T
    input_bwd = gate_pre[:, 2].T[:, ::-1]
    keep_bwd = jax.nn.log_sigmoid(gate_pre[:, 3] + forget_level[:, 1]).T[:, ::-1]
    rev_q = rec_q[:, ::-1]
    rev_k = rec_k[:, ::-1]
    rev_v = rec_v[:, ::-1]
    identity = (
        jnp.zeros((rec_heads, MK, MV), f32),
        jnp.zeros((rec_heads, MK), f32),
        jnp.full((rec_heads,), NEG, f32),
        jnp.zeros((rec_heads,), f32),
    )
    own_fwd = summary(rec_k, rec_v, input_fwd, keep_fwd)
    own_bwd = summary(rev_k, rev_v, input_bwd, keep_bwd)
    prefix_state = carried_in(own_fwd, SP, combine, identity, False)
    suffix_state = carried_in(own_bwd, SP, combine, identity, True)
    zero_heads = jnp.zeros((rec_heads,), f32)
    start_fwd = combine((init_state[0], init_norm[0], zero_heads, zero_heads), prefix_state)
    start_bwd = combine((init_state[1], init_norm[1], zero_heads, zero_heads), suffix_state)
    forward_h = recurrence(
        rec_q,
        rec_k,
        rec_v,
        input_fwd,
        keep_fwd,
        start_fwd[0],
        start_fwd[1],
        start_fwd[2],
        floor_value,
    )
    backward_h = recurrence(
        rev_q,
        rev_k,
        rev_v,
        input_bwd,
        keep_bwd,
        start_bwd[0],
        start_bwd[1],
        start_bwd[2],
        floor_value,
    )[:, ::-1]
    summed = (forward_h + backward_h).transpose(1, 0, 2)
    recurrent_out = (
        rms_rows(summed, head_gain.reshape(rec_heads, MV))
        .astype(bf16)
        .reshape(seq_rows, rec_heads * MV)
    )
    mixed_out = summed_on_arrival(
        (
            jnp.dot(attention_out, out_attn, preferred_element_type=f32)
            + jnp.dot(recurrent_out, out_rec, preferred_element_type=f32)
        ).astype(jnp.bfloat16),
        "tp",
        0,
    )
    return mixed_out.astype(bf16)


def solution(mesh):
    split = Mesh(mesh.devices.reshape(16, 4, 2, mesh.shape["tp"]), ("sp_0", "sp_1", "sp_2", "tp"))
    in_specs = (
        P(SP_TP, None),
        P(),
        P(),
        P(),
        P(),
        P(),
        P(),
        P(None, "tp"),
        P(None, "tp"),
        P(None, "tp"),
        P(None, "tp"),
        P(None, "tp"),
        P(None, "tp"),
        P(None, "tp"),
        P(None, None, "tp"),
        P(SP, None, "tp"),
        P("tp"),
        P(None, "tp", None, None),
        P(None, "tp", None),
        P("tp", None),
        P("tp", None),
    )
    out_specs = P(SP_TP, None)
    return jax.shard_map(
        shards, mesh=split, in_specs=in_specs, out_specs=out_specs, check_vma=False
    )
```

profile of v0, /device:TPU:2, one launch (start us, length us, event | category | flops | bytes accessed | tf_op | source)
XLA Modules:
  0.0 357.2 jit_solution(14680423642614228547)
XLA Ops:
  9.6 4.5 %all-to-all-start = ((bf16[4,32,2048]{2,1,0:T(8,128)(2,1)}), bf16[4,32,2048]{2,1,0:T(8,128)(2,1)S(1)}, u32[]{:S(2)}, u32[]{:S(2)}) async-start(bf16[4,32,2048]{2,1,0:T(8,128)(2,1)} %broadcast_in_dim.55), calls=%async_computation | async-start | bytes 1048576 | tf_op jit(solution)/shard_map/all_to_all | solution.py:32
  14.2 9.4 %all-to-all-done = bf16[4,32,2048]{2,1,0:T(8,128)(2,1)S(1)} async-done(((bf16[4,32,2048]{2,1,0:T(8,128)(2,1)}), bf16[4,32,2048]{2,1,0:T(8,128)(2,1)S(1)}, u32[]{:S(2)}, u32[]{:S(2)}) %all-to-all-start) | async-done | bytes 524320 | tf_op jit(solution)/shard_map/all_to_all | solution.py:32
  32.2 1.4 convolution_bitcast_fusion.4
  36.3 1.9 all-gather.6
  50.9 1.9 all-gather.9
  59.6 12.3 %all-gather.10 = f32[4,67,128]{2,1,0:T(8,128)S(1)} all-gather(f32[1,67,128]{2,1,0:T(8,128)S(1)} %maximum_bitcast_fusion.4), channel_id=6, replica_groups=mesh['sp_0'=16,'sp_1'=4,'sp_2'=2,'tp'=4] {'sp_1'}, dimensions={0}, use_global_device_ids=true | all-gather | bytes 171520 | tf_op jit(solution)/shard_map/all_gather | solution.py:62
  82.7 12.0 %all-gather.7 = f32[4,67,128]{2,1,0:T(8,128)S(1)} all-gather(f32[1,67,128]{2,1,0:T(8,128)S(1)} %maximum_bitcast_fusion.1), channel_id=3, replica_groups=mesh['sp_0'=16,'sp_1'=4,'sp_2'=2,'tp'=4] {'sp_1'}, dimensions={0}, use_global_device_ids=true | all-gather | bytes 171520 | tf_op jit(solution)/shard_map/all_gather | solution.py:62
  108.2 40.1 %all-gather.8 = f32[16,67,128]{2,1,0:T(8,128)S(1)} all-gather(f32[1,67,128]{2,1,0:T(8,128)S(1)} %maximum_bitcast_fusion.2), channel_id=4, replica_groups=mesh['sp_0'=16,'sp_1'=4,'sp_2'=2,'tp'=4] {'sp_0'}, dimensions={0}, use_global_device_ids=true | all-gather | bytes 583168 | tf_op jit(solution)/shard_map/all_gather | solution.py:62
  193.9 30.1 %all-gather.11 = f32[16,67,128]{2,1,0:T(8,128)S(1)} all-gather(f32[1,67,128]{2,1,0:T(8,128)S(1)} %maximum_bitcast_fusion.5), channel_id=7, replica_groups=mesh['sp_0'=16,'sp_1'=4,'sp_2'=2,'tp'=4] {'sp_0'}, dimensions={0}, use_global_device_ids=true | all-gather | bytes 583168 | tf_op jit(solution)/shard_map/all_gather | solution.py:62
  281.6 4.6 %slice.1142 = bf16[16384,128]{0,1:T(8,128)(2,1)} slice(bf16[16384,192]{0,1:T(8,128)(2,1)} %all-gather.14.cloned.1.call-done), slice={[0:16384], [0:128]} | slice | bytes 8388608 | tf_op jit(solution)/shard_map/slice | solution.py:43
  286.2 6.4 %copy.66 = bf16[16384,128]{1,0:T(8,128)(2,1)} copy(bf16[16384,128]{0,1:T(8,128)(2,1)} %slice.1142) | data formatting | bytes 8388608
  292.6 3.1 slice.1143
  295.7 4.8 %copy.67 = bf16[16384,64]{1,0:T(8,128)(2,1)} copy(bf16[16384,64]{0,1:T(8,128)(2,1)} %slice.1143) | data formatting | bytes 4194304
  300.5 36.8 %while.3 = (s32[]{:T(128)}, f32[128]{0:T(128)S(1)}, f32[128]{0:T(128)S(1)}, f32[128,128]{1,0:T(8,128)S(1)}, bf16[8,2048,128]{2,1,0:T(8,128)(2,1)}, /*index=5*/bf...) while((s32[]{:T(128)}, f32[128]{0:T(128)S(1)}, ...), condition=%wide.region_6.7_spmd.clone, body=%wide.region_3.6_spmd.clone.sunk | while | flops 169656960 | bytes 7004293 | solution.py:297
  301.9 1.5 fusion.711
  303.7 1.4 convolution_add_fusion.4
  306.5 1.5 fusion.711
  308.3 1.4 convolution_add_fusion.4
  311.1 1.5 fusion.711
  312.9 1.4 convolution_add_fusion.4
  315.6 1.5 fusion.711
  317.4 1.4 convolution_add_fusion.4
  320.2 1.5 fusion.711
  322.0 1.4 convolution_add_fusion.4
  324.8 1.5 fusion.711
  326.6 1.4 convolution_add_fusion.4
  329.4 1.5 fusion.711
  331.2 1.4 convolution_add_fusion.4
  334.0 1.5 fusion.711
  335.8 1.4 convolution_add_fusion.4
  337.7 1.4 fusion.18
  339.2 10.5 %all_to_all.10 = bf16[4,32,2048]{2,1,0:T(8,128)(2,1)S(1)} all-to-all(bf16[4,32,2048]{2,1,0:T(8,128)(2,1)S(1)} %bitcast.564), channel_id=1, replica_groups=mesh['sp_0'=16,'sp_1'=4,'sp_2'=2,'tp'=4] {'tp'}, dimensions={0} | all-to-all | bytes 1048576 | tf_op jit(solution)/shard_map/all_to_all | solution.py:93
  (183 shorter events, 56.6 us)
Async XLA Ops:
  6.5 22.8 %copy-start = (bf16[2048,256]{1,0:T(8,128)(2,1)S(1)}, bf16[2048,256]{1,0:T(8,128)(2,1)}, u32[]{:S(2)}) copy-start(bf16[2048,256]{1,0:T(8,128)(2,1)} %param.25) | copy-start | bytes 3145732
  6.5 22.1 %copy-start.1 = (bf16[2048,128]{1,0:T(8,128)(2,1)S(1)}, bf16[2048,128]{1,0:T(8,128)(2,1)}, u32[]{:S(2)}) copy-start(bf16[2048,128]{1,0:T(8,128)(2,1)} %param.36) | copy-start | bytes 1572868
  6.5 22.4 %copy-start.2 = (bf16[2048,128]{1,0:T(8,128)(2,1)S(1)}, bf16[2048,128]{1,0:T(8,128)(2,1)}, u32[]{:S(2)}) copy-start(bf16[2048,128]{1,0:T(8,128)(2,1)} %param.27) | copy-start | bytes 1572868
  6.5 23.2 %copy-start.7 = (f32[256]{0:T(256)S(1)}, f32[256]{0:T(256)}, u32[]{:S(2)}) copy-start(f32[256]{0:T(256)} %param.26) | copy-start | bytes 3076
  6.5 23.2 %copy-start.6 = (bf16[256,64]{0,1:T(8,128)(2,1)S(1)}, bf16[256,64]{0,1:T(8,128)(2,1)}, u32[]{:S(2)}) copy-start(bf16[256,64]{0,1:T(8,128)(2,1)} %param.31) | copy-start | bytes 98308
  8.8 21.2 %copy-start.12 = (f32[128]{0:T(128)S(1)}, f32[128]{0:T(128)}, u32[]{:S(2)}) copy-start(f32[128]{0:T(128)} %param.28) | copy-start | bytes 1540
  9.6 13.9 %all-to-all-start = ((bf16[4,32,2048]{2,1,0:T(8,128)(2,1)}), bf16[4,32,2048]{2,1,0:T(8,128)(2,1)S(1)}, u32[]{:S(2)}, u32[]{:S(2)}) async-start(bf16[4,32,2048]{2,1,0:T(8,128)(2,1)} %broadcast_in_dim.55), calls=%async_computation | async-start | bytes 1048576 | tf_op jit(solution)/shard_map/all_to_all | solution.py:32
  14.1 267.5 %all-gather.14.cloned.1.call-start = ((), (), s32[]{:S(2)}) async-start(), calls=%async_computation.2 | async-start | bytes 6340608 | tf_op jit(solution)/shard_map/all_gather | solution.py:41
  29.7 6.6 %copy-start.10 = (f32[128]{0:T(128)}, f32[128]{0:T(128)S(1)}, u32[]{:S(2)}) copy-start(f32[128]{0:T(128)S(1)} %add_rsqrt_fusion.1) | copy-start | bytes 1540
  38.2 44.5 %copy-start.8 = (f32[2,1,128]{2,1,0:T(1,128)}, f32[2,1,128]{2,1,0:T(1,128)S(1)}, u32[]{:S(2)}) copy-start(f32[2,1,128]{2,1,0:T(1,128)S(1)} %get-tuple-element.201) | copy-start | bytes 3076
  45.1 3.7 %copy-start.11 = (f32[1,128]{1,0:T(1,128)}, f32[1,128]{1,0:T(1,128)S(1)}, u32[]{:S(2)}) copy-start(f32[1,128]{1,0:T(1,128)S(1)} %rev.14) | copy-start | bytes 1540
  52.8 29.9 %copy-start.4 = (f32[2,67,128]{2,1,0:T(8,128)}, f32[2,67,128]{2,1,0:T(8,128)S(1)}, u32[]{:S(2)}) copy-start(f32[2,67,128]{2,1,0:T(8,128)S(1)} %all-gather.9) | copy-start | bytes 205828
  52.8 6.8 %copy-start.9 = (f32[2,1,128]{2,1,0:T(1,128)}, f32[2,1,128]{2,1,0:T(1,128)S(1)}, u32[]{:S(2)}) copy-start(f32[2,1,128]{2,1,0:T(1,128)S(1)} %get-tuple-element.204) | copy-start | bytes 3076
  107.7 0.5 copy-start.13
  193.4 0.5 copy-start.14
  300.5 36.8 %copy-start.3 = (bf16[128,2048]{1,0:T(8,128)(2,1)S(1)}, bf16[128,2048]{1,0:T(8,128)(2,1)}, u32[]{:S(2)}) copy-start(bf16[128,2048]{1,0:T(8,128)(2,1)} %param.42) | copy-start | bytes 1572868
  300.5 36.8 %copy-start.5 = (bf16[128,128]{1,0:T(8,128)(2,1)S(1)}, bf16[128,128]{1,0:T(8,128)(2,1)}, u32[]{:S(2)}) copy-start(bf16[128,128]{1,0:T(8,128)(2,1)} %param.33) | copy-start | bytes 98308
  300.5 37.3 %copy-start.15 = (f32[128]{0:T(128)S(1)}, f32[128]{0:T(128)}, u32[]{:S(2)}) copy-start(f32[128]{0:T(128)} %param.39) | copy-start | bytes 1540
Sparse Core Ops, SparseCore 0:
  30.9 145.1 all-gather.13
where the time goes:
time: 361 us; the launch traced here: 357 us
  between operations  133 us (37%)
  blocking collectives  109 us (30%)
  matrix products  52.7 us (15%)
  local copies, waits for them, and re-layouts  33.6 us (9%)
  other arithmetic  15.1 us (4%)
  waiting for transfers between devices  9.39 us (3%)
  starting transfers between devices  4.47 us (1%)
    all_gather x6, blocking collectives, collected_together(): both, at, found = (lax.all_gather(jnp.concatenate(lines), axis), 0, {})  98.2 us
    unnamed x35, local copies, waits for them, and re-layouts  12.3 us
    dot_general x8, matrix products, one_block(): lax.dot_general(rope_rows, rot_block, contract, preferred_element_type=f32)  11.8 us
    dot_general x8, matrix products, one_block(): jnp.dot(expo_all.astype(bf16), lat_block, preferred_element_type=f32)  11.3 us
    dot_general x8, matrix products, one_block(): lax.dot_general(abs_rows, lat_block, contract, preferred_element_type=f32)  10.8 us
    all_to_all x1, blocking collectives, summed_on_arrival(): lax.all_to_all(blocks, axis, split_axis=0, concat_axis=0, tiled=True)  10.5 us
    all_to_all x1, waiting for transfers between devices, from_everyone(): return lax.all_to_all(copies, axis, split_axis=0, concat_axis=0, tiled=True)  9.36 us
    slice x2, local copies, waits for them, and re-layouts, sent_together(): lax.slice_in_dim(filled, at, at + a.shape[along], axis=along)  7.66 us
  transfers between devices with their start and end apart: 2, of which 1 were waited for; matrix products, arithmetic and copies ran while one was open for 9% of the time, Pallas kernels for 0%

commit v1 on v0

v1 whole, which is shorter than its diff:
```python
import functools
import math

import jax
import jax.numpy as jnp
import numpy as np
from jax import lax
from jax.experimental import pallas as pl
from jax.experimental.pallas import tpu as pltpu
from jax.sharding import Mesh
from jax.sharding import PartitionSpec as P

NOPE = 128
ROPE = 64
MK = 64
EPS = 1e-06
NEG = -1e30
MESH_ID = pl.DeviceIdType.MESH
SP = ("z", "x", "c")
SP_TP = ("z", "x", "c", "y")
F32 = jnp.float32
BF16 = jnp.bfloat16
HIGHEST = lax.Precision.HIGHEST


def nn(a, b, precision=None):
    return lax.dot_general(a, b, (((1,), (0,)), ((), ())), precision=precision, preferred_element_type=F32)


def nt(a, b):
    return lax.dot_general(a, b, (((1,), (1,)), ((), ())), preferred_element_type=F32)


def rms(values, gains):
    return values * lax.rsqrt(jnp.mean(values * values, axis=-1, keepdims=True) + EPS) * gains


def rotated(values, cos, sin):
    half = values.shape[-1] // 2
    turned = jnp.concatenate([-values[:, half:], values[:, :half]], axis=-1)
    return values * cos + turned * sin


def log_sigmoid(x):
    e = jnp.exp(-jnp.abs(x))
    log1p = jnp.where(e < 1e-3, e * (1.0 - e * (0.5 - e * (1.0 / 3.0))), jnp.log(1.0 + e))
    return jnp.minimum(x, 0.0) - log1p


def combine(early, late):
    c_e, n_e, m_e, f_e = early
    c_l, n_l, m_l, f_l = late
    peak = jnp.maximum(f_l + m_e, m_l)
    kept = jnp.exp(f_l + m_e - peak)
    fresh = jnp.exp(m_l - peak)
    return (kept * c_e + fresh * c_l, kept * n_e + fresh * n_l, peak, f_e + f_l)


def read_state(ref, at, lo, sr):
    tail = ref[at, lo + sr : lo + sr + 8, :]
    return (ref[at, lo : lo + sr, :], tail[0:1], tail[1:2], tail[2:3])


def write_state(ref, at, lo, sr, state):
    c, n, m, f = state
    ref[at, lo : lo + sr, :] = c
    ref[at, lo + sr : lo + sr + 8, :] = jnp.concatenate([n, m, f, jnp.zeros((5, 128), F32)], axis=0)


def rdma(src, dst, send, recv, where):
    return pltpu.make_async_remote_copy(
        src_ref=src, dst_ref=dst, send_sem=send, recv_sem=recv, device_id=where, device_id_type=MESH_ID
    )


def body(
    sizes,
    rows_ref, in_gain_ref, query_gain_ref, kv_gain_ref, gates_ref, forget_ref, head_gain_ref, init_c_ref, init_n_ref,
    block_tab_ref, row_tab_ref,
    qd_hbm, kvd_hbm, ropet_hbm, nope_hbm, rupt_hbm, kup_hbm, vup_hbm, rq_hbm, rk_hbm, rv_hbm, oa_hbm, or_hbm,
    out_ref,
    wqd, wkv, wrope, wnope, wrup, wkup, wvup, wt, wv, wout,
    nb, kb, qb, qa_s, qb_s, ss, mx, acc, lsum, acc2, sa, ra, pfx, tb, rb, sc, rc, po, pst, rp, rst, ob, ro,
    wsem, ny_s, ny_r, kz_s, kz_r, kx_s, kx_r, kc_s, kc_r, a_s, a_r, b_s, b_r, c_s, c_r, q_s, q_r, p_s, p_r, t_s, t_r, o_s, o_r,
):
    NZ, NX, NC, NY = sizes
    G = NX * NC
    SR = MK // G
    ST = SR + 8
    T = nb.shape[0]
    R = T // NY
    H = R // 2
    zi, xi, ci, yi = (lax.axis_index(a) for a in ("z", "x", "c", "y"))
    me = xi * NC + ci
    seq = NZ * NX * NC * T
    floor_value = float(seq) ** 0.5

    barrier = pltpu.get_barrier_semaphore()
    peers = 0
    for d in range(1, NY):
        pl.semaphore_signal(barrier, inc=1, device_id={"y": lax.rem(yi + d, NY)}, device_id_type=MESH_ID)
        peers += 1
    for d in range(1, NZ):
        pl.semaphore_signal(barrier, inc=1, device_id={"z": lax.rem(zi + d, NZ)}, device_id_type=MESH_ID)
        peers += 1
    for d in range(1, G):
        g = lax.rem(me + d, G)
        pl.semaphore_signal(barrier, inc=1, device_id={"x": g // NC, "c": lax.rem(g, NC)}, device_id_type=MESH_ID)
        peers += 1

    loads = [
        pltpu.make_async_copy(src, dst, wsem.at[i])
        for i, (src, dst) in enumerate(
            [
                (kvd_hbm, wkv), (ropet_hbm, wrope), (rk_hbm, wt.at[0:MK]), (rq_hbm, wt.at[MK : 2 * MK]), (rv_hbm, wv),
                (qd_hbm, wqd), (nope_hbm, wnope), (rupt_hbm, wrup), (kup_hbm, wkup), (vup_hbm, wvup),
                (oa_hbm, wout.at[0:128]), (or_hbm, wout.at[128:256]),
            ]
        )
    ]
    for c in loads:
        c.start()

    normed = rms(rows_ref[...].astype(F32), in_gain_ref[...]).astype(BF16)
    own_rows = pl.ds(pl.multiple_of(yi * R, R), R)
    nb[own_rows, :] = normed
    wt[2 * MK : 2 * MK + 16, :] = jnp.concatenate(
        [gates_ref[...], jnp.zeros((12, gates_ref.shape[1]), BF16)], axis=0
    )
    pl.semaphore_wait(barrier, peers)

    def to_y(d, src, dst, send, recv):
        return rdma(src, dst, send.at[d], recv.at[d], {"y": lax.rem(yi + d, NY)})

    ny = [to_y(d, nb.at[own_rows], nb.at[own_rows], ny_s, ny_r) for d in range(1, NY)]
    for c in ny:
        c.start()

    sp_index = (zi * NX + xi) * NC + ci
    block_row = block_tab_ref[pl.ds(sp_index, 1), :]
    cos_b, sin_b = block_row[:, :ROPE], block_row[:, ROPE:]

    def angles(table):
        cos_r, sin_r = table[:, :ROPE], table[:, ROPE:]
        return cos_b * cos_r - sin_b * sin_r, sin_b * cos_r + cos_b * sin_r

    loads[0].wait()
    loads[1].wait()
    latent = rms(nn(normed, wkv[...]), kv_gain_ref[...]).astype(BF16)
    rope = rotated(nt(normed, wrope[...]), *angles(row_tab_ref[own_rows, :])).astype(BF16)
    own_chunk = pl.ds(pl.multiple_of(zi * H, H), H)
    kb[me, own_chunk, :] = jnp.concatenate([latent[:H], rope[:H], rope[H:], latent[H:]], axis=1)

    def z_key(d, slot):
        rows = pl.ds(pl.multiple_of(slot * H, H), H)
        return rdma(
            kb.at[me, rows], kb.at[me, rows], kz_s.at[d], kz_r.at[d], {"z": lax.rem(zi + d, NZ)}
        )

    def start_z_key(d, _):
        z_key(d, zi).start()
        return 0

    lax.fori_loop(1, NZ, start_z_key, 0)

    for i in (2, 3, 4, 5):
        loads[i].wait()
    for d in range(1, NY):
        rows = pl.ds(pl.multiple_of(lax.rem(yi - d + NY, NY) * R, R), R)
        to_y(d, nb.at[rows], nb.at[rows], ny_s, ny_r).wait_recv()
    kqg = nt(wt[...], nb[...])
    v = nn(nb[...], wv[...]).astype(BF16)
    kq_t = jnp.transpose(kqg[0 : 2 * MK])
    k_t = kqg[0:MK].astype(BF16)
    kq = kq_t.astype(BF16)
    i_f = kqg[2 * MK : 2 * MK + 1]
    i_b = kqg[2 * MK + 2 : 2 * MK + 3]
    f_f = log_sigmoid(kqg[2 * MK + 1 : 2 * MK + 2] + forget_ref[0:1, :])
    f_b = log_sigmoid(kqg[2 * MK + 3 : 2 * MK + 4] + forget_ref[1:2, :])
    row_id = lax.broadcasted_iota(jnp.int32, (T, T), 0)
    col_id = lax.broadcasted_iota(jnp.int32, (T, T), 1)
    upto = row_id <= col_id
    after = row_id >= col_id
    logs = jnp.concatenate([f_f, f_b, jnp.zeros((6, T), F32)], axis=0)
    cum_f = nn(logs, upto.astype(F32), HIGHEST)[0:1]
    cum_b = nn(logs, after.astype(F32), HIGHEST)[1:2]
    cums = jnp.transpose(jnp.concatenate([cum_f, cum_b, jnp.zeros((6, T), F32)], axis=0))
    cum_f_col, cum_b_col = cums[:, 0:1], cums[:, 1:2]
    in_f, in_b = i_f - cum_f, i_b - cum_b
    end_f, end_b = cum_f[:, T - 1 : T], cum_b[:, 0:1]
    peak_f = jnp.max(end_f + in_f, axis=1, keepdims=True)
    peak_b = jnp.max(end_b + in_b, axis=1, keepdims=True)
    w_f = jnp.exp(end_f + in_f - peak_f)
    w_b = jnp.exp(end_b + in_b - peak_b)
    k_scaled = k_t.astype(F32) * (MK ** -0.5)
    weighted = jnp.concatenate([k_scaled * w_f, k_scaled * w_b], axis=0).astype(BF16)
    memory = nn(weighted, v)
    weights = jnp.concatenate([w_f, w_b, jnp.zeros((6, T), F32)], axis=0).astype(BF16)
    norms = nn(weights, kq) * (MK ** -0.5)
    spread = jnp.zeros((1, 128), F32)
    tail_f = (norms[0:1], peak_f + spread, end_f + spread)
    tail_b = (norms[1:2], peak_b + spread, end_b + spread)
    for g in range(G):
        write_state(sa, g, 0, SR, (memory[g * SR : (g + 1) * SR], *tail_f))
        write_state(sa, g, ST, SR, (memory[MK + g * SR : MK + (g + 1) * SR], *tail_b))

    def to_group(d, src, dst, send, recv):
        g = lax.rem(me + d, G)
        return rdma(src, dst, send.at[d], recv.at[d], {"x": g // NC, "c": lax.rem(g, NC)})

    stage_a = [to_group(d, sa.at[lax.rem(me + d, G)], ra.at[me], a_s, a_r) for d in range(1, G)]
    for c in stage_a:
        c.start()
    ra[me] = sa[me]

    for i in (6, 7, 8):
        loads[i].wait()
    q_latent = rms(nn(nb[...], wqd[...]), query_gain_ref[...]).astype(BF16)
    q_nope = nn(q_latent, wnope[...]).astype(BF16)
    q_abs = nt(q_nope, wkup[...]).astype(BF16)
    q_rope = rotated(nt(q_latent, wrup[...]), *angles(row_tab_ref[...])).astype(BF16)
    qb[yi] = jnp.concatenate([q_abs, q_rope, q_rope], axis=1)
    stage_q = [to_y(d, qb.at[yi], qb.at[yi], q_s, q_r) for d in range(1, NY)]
    for c in stage_q:
        c.start()

    def wait_z_key(d, _):
        z_key(d, lax.rem(zi - d + NZ, NZ)).wait_recv()
        return 0

    lax.fori_loop(1, NZ, wait_z_key, 0)

    def x_key(d, g):
        return rdma(kb.at[g], kb.at[g], kx_s.at[d], kx_r.at[d], {"x": lax.rem(xi + d, NX)})

    def c_key(d, g):
        return rdma(kb.at[g], kb.at[g], kc_s.at[d], kc_r.at[d], {"c": 1 - ci})

    stage_x = [x_key(d, me) for d in range(1, NX)]
    for c in stage_x:
        c.start()
    stage_k = [c_key(0, me)]
    stage_k[0].start()

    scores = nt(kq[:, MK : 2 * MK], kq[:, 0:MK]) * (MK ** -0.5)
    log_f = jnp.where(after, cum_f_col + in_f, NEG)
    log_b = jnp.where(upto, cum_b_col + in_b, NEG)
    max_f = jnp.max(log_f, axis=1, keepdims=True)
    max_b = jnp.max(log_b, axis=1, keepdims=True)
    gated_f = scores * jnp.exp(log_f - max_f)
    gated_b = scores * jnp.exp(log_b - max_b)
    num_f = nn(gated_f.astype(BF16), v)
    num_b = nn(gated_b.astype(BF16), v)
    den_f = jnp.sum(gated_f, axis=1, keepdims=True)
    den_b = jnp.sum(gated_b, axis=1, keepdims=True)

    for d in range(1, G):
        g = lax.rem(me - d + G, G)
        to_group(d, sa.at[me], ra.at[g], a_s, a_r).wait_recv()
    zero = (jnp.zeros((SR, 128), F32), spread, spread + NEG, spread)
    run = zero
    for g in range(G):
        write_state(pfx, g, 0, SR, run)
        run = combine(run, read_state(ra, g, 0, SR))
    write_state(tb, 0, 0, SR, run)
    run = zero
    for g in reversed(range(G)):
        write_state(pfx, g, ST, SR, run)
        run = combine(run, read_state(ra, g, ST, SR))
    write_state(tb, 1, 0, SR, run)

    def z_total(d, slot):
        return rdma(tb.at[(zi + d) // NZ], rb.at[slot], b_s.at[d], b_r.at[d], {"z": lax.rem(zi + d, NZ)})

    def start_z_total(d, _):
        z_total(d, zi).start()
        return 0

    lax.fori_loop(1, NZ, start_z_total, 0)

    for d in range(1, NY):
        slot = lax.rem(yi - d + NY, NY)
        to_y(d, qb.at[slot], qb.at[slot], q_s, q_r).wait_recv()
    lane = lax.broadcasted_iota(jnp.int32, (T, 128), 1)
    for h in range(NY):
        q_h = qb[h]
        rr = q_h[:, 128:256].astype(F32)
        first = jnp.where(lane < ROPE, rr, 0.0).astype(BF16)
        second = jnp.where(lane < ROPE, 0.0, rr).astype(BF16)
        qa_s[h * T : (h + 1) * T, :] = jnp.concatenate([q_h[:, 0:128], first], axis=1)
        qb_s[h * T : (h + 1) * T, :] = jnp.concatenate([second, q_h[:, 0:128]], axis=1)
    for d in range(1, NX):
        g = lax.rem(xi - d + NX, NX) * NC + ci
        x_key(d, g).wait_recv()
        stage_k.append(c_key(d, g))
        stage_k[-1].start()

    scale = (NOPE + ROPE) ** -0.5
    KEYS = kb.shape[1]

    def lane_max(s):
        parts = [s[:, i : i + 128] for i in range(0, s.shape[1], 128)]
        return functools.reduce(jnp.maximum, parts)

    def lane_sum(s):
        parts = [s[:, i : i + 128] for i in range(0, s.shape[1], 128)]
        return functools.reduce(jnp.add, parts)

    def share(core, total):
        mx[...] = jnp.full(mx.shape, NEG, F32)

        def look(i, _):
            g = i * NC + core
            s_a = nt(qa_s[...], kb[g, :, 0:256])
            ss[2 * i] = s_a
            s_b = nt(qb_s[...], kb[g, :, 128:384])
            ss[2 * i + 1] = s_b
            mx[...] = jnp.maximum(mx[...], jnp.maximum(lane_max(s_a), lane_max(s_b)))
            return 0

        lax.fori_loop(0, NX, look, 0)
        top = jnp.max(mx[...], axis=1, keepdims=True)
        total[...] = jnp.zeros(total.shape, F32)
        lsum[...] = jnp.zeros(lsum.shape, F32)

        def add(i, _):
            g = i * NC + core
            p_a = jnp.exp((ss[2 * i] - top) * scale)
            p_b = jnp.exp((ss[2 * i + 1] - top) * scale)
            lsum[...] += lane_sum(p_a) + lane_sum(p_b)
            total[...] += nn(p_a.astype(BF16), kb[g, :, 0:128]) + nn(p_b.astype(BF16), kb[g, :, 256:384])
            return 0

        lax.fori_loop(0, NX, add, 0)
        return top, jnp.sum(lsum[...], axis=1, keepdims=True)

    top_1, sum_1 = share(ci, acc)

    def wait_z_total(d, _):
        z_total(d, lax.rem(zi - d + NZ, NZ)).wait_recv()
        return 0

    lax.fori_loop(1, NZ, wait_z_total, 0)
    own_slice = pl.ds(pl.multiple_of(me * SR, SR), SR)
    pad = jnp.zeros((1, 128 - MK), F32)

    def initial(way):
        norm = jnp.concatenate([init_n_ref[way : way + 1, :], pad], axis=1)
        return (init_c_ref[way, own_slice, :], norm, spread, spread)

    run_f = lax.fori_loop(0, zi, lambda j, run: combine(run, read_state(rb, j, 0, SR)), initial(0))
    run_b = lax.fori_loop(
        0, NZ - 1 - zi, lambda j, run: combine(run, read_state(rb, NZ - 1 - j, 0, SR)), initial(1)
    )
    for g in range(G):
        write_state(sc, g, 0, SR, combine(run_f, read_state(pfx, g, 0, SR)))
        write_state(sc, g, ST, SR, combine(run_b, read_state(pfx, g, ST, SR)))
    stage_c = [to_group(d, sc.at[lax.rem(me + d, G)], rc.at[me], c_s, c_r) for d in range(1, G)]
    for c in stage_c:
        c.start()
    rc[me] = sc[me]

    for d in range(NX):
        g = lax.rem(xi - d + NX, NX) * NC + 1 - ci
        c_key(d, g).wait_recv()
    top_2, sum_2 = share(1 - ci, acc2)

    top = jnp.maximum(top_1, top_2)
    part_1 = jnp.exp((top_1 - top) * scale)
    part_2 = jnp.exp((top_2 - top) * scale)
    mass = part_1 * sum_1 + part_2 * sum_2
    partial = (part_1 * acc[...] + part_2 * acc2[...]) / mass
    log_mass = top * scale + jnp.log(mass)
    for h in range(NY):
        po[h] = partial[h * T : (h + 1) * T].astype(BF16)
        pst[h] = jnp.transpose(jnp.broadcast_to(log_mass[h * T : (h + 1) * T], (T, 128)))[0:8]
    stage_p = [to_y(d, po.at[lax.rem(yi + d, NY)], rp.at[yi], p_s, p_r) for d in range(1, NY)]
    stage_t = [to_y(d, pst.at[lax.rem(yi + d, NY)], rst.at[yi], t_s, t_r) for d in range(1, NY)]
    for c in stage_t + stage_p:
        c.start()
    rp[yi] = po[yi]
    rst[yi] = pst[yi]

    for d in range(1, G):
        g = lax.rem(me - d + G, G)
        to_group(d, sc.at[me], rc.at[g], c_s, c_r).wait_recv()
    state_f = jnp.concatenate([rc[g, 0:SR, :] for g in range(G)], axis=0)
    state_b = jnp.concatenate([rc[g, ST : ST + SR, :] for g in range(G)], axis=0)
    tail_f = rc[0, SR : SR + 8, :]
    tail_b = rc[0, ST + SR : ST + SR + 8, :]
    query = kq[:, MK : 2 * MK]
    carried = nn(query, jnp.concatenate([state_f, state_b], axis=1).astype(BF16))
    query32 = query.astype(F32)

    def finished(num, den, row_max, cum_col, from_state, tail):
        carry_log = cum_col + tail[1:2, 0:1]
        new_max = jnp.maximum(row_max, carry_log)
        inside = jnp.exp(row_max - new_max)
        outside = jnp.exp(carry_log - new_max)
        from_norm = jnp.sum(query32 * tail[0:1, 0:MK], axis=1, keepdims=True)
        below = inside * den + outside * from_norm
        above = inside * num + outside * from_state
        return above / jnp.maximum(jnp.abs(below), floor_value * jnp.exp(-new_max))

    both = finished(num_f, den_f, max_f, cum_f_col, carried[:, 0:128], tail_f) + finished(
        num_b, den_b, max_b, cum_b_col, carried[:, 128:256], tail_b
    )
    recurrent = rms(both, head_gain_ref[...]).astype(BF16)

    for d in range(1, NY):
        slot = lax.rem(yi - d + NY, NY)
        to_y(d, po.at[slot], rp.at[slot], p_s, p_r).wait_recv()
        to_y(d, pst.at[slot], rst.at[slot], t_s, t_r).wait_recv()
    cols = [jnp.transpose(rst[h])[:, 0:1] for h in range(NY)]
    top = functools.reduce(jnp.maximum, cols)
    parts = [jnp.exp(c - top) for c in cols]
    mass = functools.reduce(jnp.add, parts)
    merged = functools.reduce(jnp.add, [p * rp[h].astype(F32) for h, p in enumerate(parts)])
    attended = (merged / mass).astype(BF16)
    for i in (9, 10, 11):
        loads[i].wait()
    attention = nn(attended, wvup[...]).astype(BF16)
    joined = jnp.concatenate([attention, recurrent], axis=1)
    ob[...] = nn(joined, wout[...]).astype(BF16)

    def rows_of(y):
        return pl.ds(pl.multiple_of(y * R, R), R)

    stage_o = [to_y(d, ob.at[rows_of(lax.rem(yi + d, NY))], ro.at[yi], o_s, o_r) for d in range(1, NY)]
    for c in stage_o:
        c.start()
    result = ob[own_rows, :].astype(F32)
    for d in range(1, NY):
        slot = lax.rem(yi - d + NY, NY)
        to_y(d, ob.at[own_rows], ro.at[slot], o_s, o_r).wait_recv()
        result = result + ro[slot].astype(F32)
    out_ref[...] = result.astype(BF16)

    for c in ny + stage_a + stage_q + stage_x + stage_k + stage_c + stage_p + stage_t + stage_o:
        c.wait_send()

    def wait_z_sends(d, _):
        z_key(d, zi).wait_send()
        z_total(d, zi).wait_send()
        return 0

    lax.fori_loop(1, NZ, wait_z_sends, 0)


def rotary_tables(blocks, rows):
    half = ROPE // 2
    frequency = 10000.0 ** (-np.arange(half, dtype=np.float64) / half)

    def table(positions):
        angle = positions[:, None] * frequency[None, :]
        return np.concatenate([np.cos(angle), np.cos(angle), np.sin(angle), np.sin(angle)], axis=1).astype(np.float32)

    return table(np.arange(blocks, dtype=np.float64) * rows), table(np.arange(rows, dtype=np.float64))


def shards(
    sizes, rows_in, in_gain, query_down, query_gain, kv_down, kv_gain, rope_down, query_nope_up, query_rope_up, key_up,
    value_up, rec_query, rec_key, rec_value, gate_weight, forget_level, head_gain, init_state, init_norm, out_attn, out_rec,
):
    NZ, NX, NC, NY = sizes
    G = NX * NC
    SR = MK // G
    ST = SR + 8
    T = forget_level.shape[0]
    R, D = rows_in.shape
    H = R // 2
    KEYS = NZ * H
    block_tab, row_tab = rotary_tables(NZ * G, T)
    vmem_args = (
        rows_in, in_gain.reshape(1, -1), query_gain.reshape(1, -1), kv_gain.reshape(1, -1), gate_weight[:, :, 0].T,
        forget_level[:, :, 0].T, head_gain.reshape(1, -1), init_state[:, 0], init_norm[:, 0],
        jnp.asarray(block_tab), jnp.asarray(row_tab),
    )
    hbm_args = (
        query_down, kv_down, rope_down.T, query_nope_up, query_rope_up.T, key_up, value_up, rec_query.T, rec_key.T,
        rec_value, out_attn, out_rec,
    )
    dma = pltpu.SemaphoreType.DMA
    return pl.pallas_call(
        functools.partial(body, sizes),
        out_shape=jax.ShapeDtypeStruct((R, D), BF16),
        in_specs=[pl.BlockSpec(memory_space=pltpu.VMEM)] * len(vmem_args)
        + [pl.BlockSpec(memory_space=pltpu.HBM)] * len(hbm_args),
        out_specs=pl.BlockSpec(memory_space=pltpu.VMEM),
        scratch_shapes=[
            *[pltpu.VMEM(a.shape, BF16) for a in hbm_args[:7]],
            pltpu.VMEM((2 * MK + 16, D), BF16),
            pltpu.VMEM(rec_value.shape, BF16),
            pltpu.VMEM((256, D), BF16),
            pltpu.VMEM((T, D), BF16),
            pltpu.VMEM((G, KEYS, 384), BF16),
            pltpu.VMEM((NY, T, 256), BF16),
            pltpu.VMEM((NY * T, 256), BF16),
            pltpu.VMEM((NY * T, 256), BF16),
            pltpu.VMEM((2 * NX, NY * T, KEYS), F32),
            pltpu.VMEM((NY * T, 128), F32),
            pltpu.VMEM((NY * T, 128), F32),
            pltpu.VMEM((NY * T, 128), F32),
            pltpu.VMEM((NY * T, 128), F32),
            pltpu.VMEM((G, 2 * ST, 128), F32),
            pltpu.VMEM((G, 2 * ST, 128), F32),
            pltpu.VMEM((G, 2 * ST, 128), F32),
            pltpu.VMEM((2, ST, 128), F32),
            pltpu.VMEM((NZ, ST, 128), F32),
            pltpu.VMEM((G, 2 * ST, 128), F32),
            pltpu.VMEM((G, 2 * ST, 128), F32),
            pltpu.VMEM((NY, T, 128), BF16),
            pltpu.VMEM((NY, 8, T), F32),
            pltpu.VMEM((NY, T, 128), BF16),
            pltpu.VMEM((NY, 8, T), F32),
            pltpu.VMEM((T, D), BF16),
            pltpu.VMEM((NY, R, D), BF16),
            dma((12,)),
            *[dma((NY,))] * 2,
            *[dma((NZ,))] * 2,
            *[dma((NX,))] * 4,
            *[dma((G,))] * 2,
            *[dma((NZ,))] * 2,
            *[dma((G,))] * 2,
            *[dma((NY,))] * 8,
        ],
        compiler_params=pltpu.CompilerParams(
            collective_id=0, has_side_effects=True, vmem_limit_bytes=48 * 1024 * 1024
        ),
        name="layer",
    )(*vmem_args, *hbm_args)


def solution(mesh):
    sp, tp = mesh.shape["sp"], mesh.shape["tp"]
    sizes = (sp // 8, 4, 2, tp)
    split = Mesh(mesh.devices.reshape(sizes), SP_TP)
    in_specs = (
        P(SP_TP, None), P(), P(), P(), P(), P(), P(),
        P(None, "y"), P(None, "y"), P(None, "y"), P(None, "y"), P(None, "y"), P(None, "y"), P(None, "y"),
        P(None, None, "y"), P(SP, None, "y"), P("y"), P(None, "y", None, None), P(None, "y", None),
        P("y", None), P("y", None),
    )
    return jax.shard_map(
        functools.partial(shards, sizes), mesh=split, in_specs=in_specs, out_specs=P(SP_TP, None), check_vma=False
    )
```

time: 361 us -> 74.3 us (0.21)
  the two profiles are of different devices: /device:TPU:2 before, /device:TPU:32 now
where the time goes in v1:
time: 74.3 us; the launch traced here: 73.4 us
  Pallas kernels  56.5 us (76%)
  local copies, waits for them, and re-layouts  16.8 us (23%)
    pallas_call x1, Pallas kernels, shards(): pl.pallas_call(functools.partial(body, sizes), out_shape=jax.ShapeDtypeSt...  56.5 us
    unnamed x47, local copies, waits for them, and re-layouts  16.8 us

profile of v1, /device:TPU:32, one launch (start us, length us, event | category | flops | bytes accessed | tf_op | source)
XLA Modules:
  0.0 73.4 jit_solution(5359224600404299036)
XLA Ops:
  0.0 0.0 copy-start.16
  0.0 0.0 copy-start.22
  0.0 0.0 copy-start.20
  0.0 0.0 copy-start.18
  0.0 0.0 copy-start.21
  0.0 0.7 copy-done.16
  0.7 0.0 copy-done.22
  0.7 0.0 copy-done.19
  0.7 0.0 copy-done.20
  0.7 0.0 copy-done.18
  0.7 0.0 copy-done.21
  0.7 0.0 copy-start
  0.8 1.2 %copy-done = bf16[2048,256]{1,0:T(8,128)(2,1)S(1)} copy-done((bf16[2048,256]{1,0:T(8,128)(2,1)S(1)}, bf16[2048,256]{1,0:T(8,128)(2,1)}, u32[]{:S(2)}) %copy-start) | copy-done | bytes 1048600
  2.0 0.0 copy-start.1
  2.0 1.0 %copy-done.1 = bf16[2048,128]{1,0:T(8,128)(2,1)S(1)} copy-done((bf16[2048,128]{1,0:T(8,128)(2,1)S(1)}, bf16[2048,128]{1,0:T(8,128)(2,1)}, u32[]{:S(2)}) %copy-start.1) | copy-done | bytes 524312
  3.0 1.0 %copy-done.2 = bf16[2048,128]{1,0:T(8,128)(2,1)S(1)} copy-done((bf16[2048,128]{1,0:T(8,128)(2,1)S(1)}, bf16[2048,128]{1,0:T(8,128)(2,1)}, u32[]{:S(2)}) %copy-start.2) | copy-done | bytes 524312
  4.1 1.0 %copy-done.3 = bf16[128,2048]{1,0:T(8,128)(2,1)S(1)} copy-done((bf16[128,2048]{1,0:T(8,128)(2,1)S(1)}, bf16[128,2048]{1,0:T(8,128)(2,1)}, u32[]{:S(2)}) %copy-start.3) | copy-done | bytes 524312
  5.1 1.0 %copy-done.4 = bf16[128,2048]{1,0:T(8,128)(2,1)S(1)} copy-done((bf16[128,2048]{1,0:T(8,128)(2,1)S(1)}, bf16[128,2048]{1,0:T(8,128)(2,1)}, u32[]{:S(2)}) %copy-start.4) | copy-done | bytes 524312
  6.1 0.9 %copy-done.5 = bf16[2048,64]{0,1:T(8,128)(2,1)S(1)} copy-done((bf16[2048,64]{0,1:T(8,128)(2,1)S(1)}, bf16[2048,64]{0,1:T(8,128)(2,1)}, u32[]{:S(2)}) %copy-start.5) | copy-done | bytes 262168
  7.1 0.9 %copy-done.6 = bf16[2048,64]{0,1:T(8,128)(2,1)S(1)} copy-done((bf16[2048,64]{0,1:T(8,128)(2,1)S(1)}, bf16[2048,64]{0,1:T(8,128)(2,1)}, u32[]{:S(2)}) %copy-start.6) | copy-done | bytes 262168
  8.0 0.9 %copy-done.7 = bf16[2048,64]{0,1:T(8,128)(2,1)S(1)} copy-done((bf16[2048,64]{0,1:T(8,128)(2,1)S(1)}, bf16[2048,64]{0,1:T(8,128)(2,1)}, u32[]{:S(2)}) %copy-start.7) | copy-done | bytes 262168
  9.0 0.9 %copy-done.8 = bf16[32,2048]{1,0:T(8,128)(2,1)S(1)} copy-done((bf16[32,2048]{1,0:T(8,128)(2,1)S(1)}, bf16[32,2048]{1,0:T(8,128)(2,1)}, u32[]{:S(2)}) %copy-start.8) | copy-done | bytes 131096
  9.9 0.8 %copy-done.9 = f32[2,1,64,128]{3,2,1,0:T(8,128)S(1)} copy-done((f32[2,1,64,128]{3,2,1,0:T(8,128)S(1)}, f32[2,1,64,128]{3,2,1,0:T(8,128)}, u32[]{:S(2)}) %copy-start.9) | copy-done | bytes 65560
  10.7 0.8 %copy-done.10 = bf16[256,128]{1,0:T(8,128)(2,1)S(1)} copy-done((bf16[256,128]{1,0:T(8,128)(2,1)S(1)}, bf16[256,128]{1,0:T(8,128)(2,1)}, u32[]{:S(2)}) %copy-start.10) | copy-done | bytes 65560
  11.6 0.8 %copy-done.11 = f32[128,128]{1,0:T(8,128)S(1)} copy-done((f32[128,128]{1,0:T(8,128)S(1)}, f32[128,128]{1,0:T(8,128)}, u32[]{:S(2)}) %copy-start.11) | copy-done | bytes 65560
  12.4 0.8 %copy-done.12 = f32[128,128]{1,0:T(8,128)S(1)} copy-done((f32[128,128]{1,0:T(8,128)S(1)}, f32[128,128]{1,0:T(8,128)}, u32[]{:S(2)}) %copy-start.12) | copy-done | bytes 65560
  13.3 0.8 %copy-done.13 = bf16[256,64]{0,1:T(8,128)(2,1)S(1)} copy-done((bf16[256,64]{0,1:T(8,128)(2,1)S(1)}, bf16[256,64]{0,1:T(8,128)(2,1)}, u32[]{:S(2)}) %copy-start.13) | copy-done | bytes 32792
  14.0 0.8 %copy-done.14 = bf16[128,128]{1,0:T(8,128)(2,1)S(1)} copy-done((bf16[128,128]{1,0:T(8,128)(2,1)S(1)}, bf16[128,128]{1,0:T(8,128)(2,1)}, u32[]{:S(2)}) %copy-start.14) | copy-done | bytes 32792
  14.8 0.8 %copy-done.15 = bf16[128,128]{1,0:T(8,128)(2,1)S(1)} copy-done((bf16[128,128]{1,0:T(8,128)(2,1)S(1)}, bf16[128,128]{1,0:T(8,128)(2,1)}, u32[]{:S(2)}) %copy-start.15) | copy-done | bytes 32792
  15.5 0.7 copy-done.17
  16.2 56.5 %layer.1 = bf16[32,2048]{1,0:T(8,128)(2,1)S(1)} custom-call(bf16[32,2048]{1,0:T(8,128)(2,1)S(1)} %copy-done.8, f32[1,2048]{1,0:T(1,128)S(1)} %bitcast.22, f32[1,256]{1,0:T(1,128)S(1)} %bitcast.23, f32[1,128]{1,0:T(1,128)S(1)} %bitcast.26, bf16[4,2048]{1,0:T(4,128)(2,1)S(1)} %bitcast.21, f32[2,128]{1,0:T(2,128)S(1)} %bitcast.24, f32[1,128]{1,0:T(1,128)S(1)} %bitcast.27, ...), custom_call_target="tpu_custom_call" | custom-call | tf_op jit(solution)/shard_map/layer/pallas_call | solution.py:484
  72.7 0.7 copy.25
  (16 shorter events, 0.0 us)
Async XLA Ops:
  0.0 0.7 copy-start.16
  0.0 0.7 copy-start.22
  0.0 0.7 copy-start.19
  0.0 0.7 copy-start.20
  0.0 0.7 copy-start.18
  0.0 0.7 copy-start.21
  0.7 1.2 %copy-start = (bf16[2048,256]{1,0:T(8,128)(2,1)S(1)}, bf16[2048,256]{1,0:T(8,128)(2,1)}, u32[]{:S(2)}) copy-start(bf16[2048,256]{1,0:T(8,128)(2,1)} %qd_hbm.1) | copy-start | bytes 3145732
  2.0 1.0 %copy-start.1 = (bf16[2048,128]{1,0:T(8,128)(2,1)S(1)}, bf16[2048,128]{1,0:T(8,128)(2,1)}, u32[]{:S(2)}) copy-start(bf16[2048,128]{1,0:T(8,128)(2,1)} %kvd_hbm.1) | copy-start | bytes 1572868
  3.0 1.0 %copy-start.2 = (bf16[2048,128]{1,0:T(8,128)(2,1)S(1)}, bf16[2048,128]{1,0:T(8,128)(2,1)}, u32[]{:S(2)}) copy-start(bf16[2048,128]{1,0:T(8,128)(2,1)} %rv_hbm.1) | copy-start | bytes 1572868
  4.1 1.0 %copy-start.3 = (bf16[128,2048]{1,0:T(8,128)(2,1)S(1)}, bf16[128,2048]{1,0:T(8,128)(2,1)}, u32[]{:S(2)}) copy-start(bf16[128,2048]{1,0:T(8,128)(2,1)} %oa_hbm.1) | copy-start | bytes 1572868
  5.1 1.0 %copy-start.4 = (bf16[128,2048]{1,0:T(8,128)(2,1)S(1)}, bf16[128,2048]{1,0:T(8,128)(2,1)}, u32[]{:S(2)}) copy-start(bf16[128,2048]{1,0:T(8,128)(2,1)} %or_hbm.1) | copy-start | bytes 1572868
  6.1 0.9 %copy-start.5 = (bf16[2048,64]{0,1:T(8,128)(2,1)S(1)}, bf16[2048,64]{0,1:T(8,128)(2,1)}, u32[]{:S(2)}) copy-start(bf16[2048,64]{0,1:T(8,128)(2,1)} %param.29) | copy-start | bytes 786436
  7.1 0.9 %copy-start.6 = (bf16[2048,64]{0,1:T(8,128)(2,1)S(1)}, bf16[2048,64]{0,1:T(8,128)(2,1)}, u32[]{:S(2)}) copy-start(bf16[2048,64]{0,1:T(8,128)(2,1)} %param.34) | copy-start | bytes 786436
  8.0 0.9 %copy-start.7 = (bf16[2048,64]{0,1:T(8,128)(2,1)S(1)}, bf16[2048,64]{0,1:T(8,128)(2,1)}, u32[]{:S(2)}) copy-start(bf16[2048,64]{0,1:T(8,128)(2,1)} %param.35) | copy-start | bytes 786436
  9.0 0.9 %copy-start.8 = (bf16[32,2048]{1,0:T(8,128)(2,1)S(1)}, bf16[32,2048]{1,0:T(8,128)(2,1)}, u32[]{:S(2)}) copy-start(bf16[32,2048]{1,0:T(8,128)(2,1)} %rows_ref.1) | copy-start | bytes 393220
  9.9 0.8 %copy-start.9 = (f32[2,1,64,128]{3,2,1,0:T(8,128)S(1)}, f32[2,1,64,128]{3,2,1,0:T(8,128)}, u32[]{:S(2)}) copy-start(f32[2,1,64,128]{3,2,1,0:T(8,128)} %param.40) | copy-start | bytes 196612
  10.7 0.8 %copy-start.10 = (bf16[256,128]{1,0:T(8,128)(2,1)S(1)}, bf16[256,128]{1,0:T(8,128)(2,1)}, u32[]{:S(2)}) copy-start(bf16[256,128]{1,0:T(8,128)(2,1)} %nope_hbm.1) | copy-start | bytes 196612
  11.6 0.8 %copy-start.11 = (f32[128,128]{1,0:T(8,128)S(1)}, f32[128,128]{1,0:T(8,128)}, u32[]{:S(2)}) copy-start(f32[128,128]{1,0:T(8,128)} %constant.5.clone.row_tab_ref) | copy-start | bytes 196612
  12.4 0.8 %copy-start.12 = (f32[128,128]{1,0:T(8,128)S(1)}, f32[128,128]{1,0:T(8,128)}, u32[]{:S(2)}) copy-start(f32[128,128]{1,0:T(8,128)} %constant.4.clone.block_tab_ref) | copy-start | bytes 196612
  13.3 0.8 %copy-start.13 = (bf16[256,64]{0,1:T(8,128)(2,1)S(1)}, bf16[256,64]{0,1:T(8,128)(2,1)}, u32[]{:S(2)}) copy-start(bf16[256,64]{0,1:T(8,128)(2,1)} %param.31) | copy-start | bytes 98308
  14.0 0.8 %copy-start.14 = (bf16[128,128]{1,0:T(8,128)(2,1)S(1)}, bf16[128,128]{1,0:T(8,128)(2,1)}, u32[]{:S(2)}) copy-start(bf16[128,128]{1,0:T(8,128)(2,1)} %kup_hbm.1) | copy-start | bytes 98308
  14.8 0.8 %copy-start.15 = (bf16[128,128]{1,0:T(8,128)(2,1)S(1)}, bf16[128,128]{1,0:T(8,128)(2,1)}, u32[]{:S(2)}) copy-start(bf16[128,128]{1,0:T(8,128)(2,1)} %vup_hbm.1) | copy-start | bytes 98308
  15.5 0.7 copy-start.17

commit v2 on v1

--- a/solution.py
+++ b/solution.py
@@ -75,10 +75,12 @@
 
 def body(
     sizes,
+    rows_hbm, in_gain_hbm, query_gain_hbm, kv_gain_hbm, gates_hbm, forget_hbm, head_gain_hbm, init_c_hbm, init_n_hbm,
+    block_tab_hbm, row_tab_hbm,
+    qd_hbm, kvd_hbm, ropet_hbm, nope_hbm, rupt_hbm, kup_hbm, vup_hbm, rq_hbm, rk_hbm, rv_hbm, oa_hbm, or_hbm,
+    out_ref,
     rows_ref, in_gain_ref, query_gain_ref, kv_gain_ref, gates_ref, forget_ref, head_gain_ref, init_c_ref, init_n_ref,
     block_tab_ref, row_tab_ref,
-    qd_hbm, kvd_hbm, ropet_hbm, nope_hbm, rupt_hbm, kup_hbm, vup_hbm, rq_hbm, rk_hbm, rv_hbm, oa_hbm, or_hbm,
-    out_ref,
     wqd, wkv, wrope, wnope, wrup, wkup, wvup, wt, wv, wout,
     nb, kb, qb, qa_s, qb_s, ss, mx, acc, lsum, acc2, sa, ra, pfx, tb, rb, sc, rc, po, pst, rp, rst, ob, ro,
     wsem, ny_s, ny_r, kz_s, kz_r, kx_s, kx_r, kc_s, kc_r, a_s, a_r, b_s, b_r, c_s, c_r, q_s, q_r, p_s, p_r, t_s, t_r, o_s, o_r,
@@ -95,6 +97,23 @@
     seq = NZ * NX * NC * T
     floor_value = float(seq) ** 0.5
 
+    plan = (
+        ("rows", rows_hbm, rows_ref), ("in_gain", in_gain_hbm, in_gain_ref), ("kv", kvd_hbm, wkv), ("rope", ropet_hbm, wrope),
+        ("kv_gain", kv_gain_hbm, kv_gain_ref), ("blocks", block_tab_hbm, block_tab_ref), ("table", row_tab_hbm, row_tab_ref),
+        ("gates", gates_hbm, gates_ref), ("rk", rk_hbm, wt.at[0:MK]), ("rq", rq_hbm, wt.at[MK : 2 * MK]),
+        ("rv", rv_hbm, wv), ("forget", forget_hbm, forget_ref), ("qd", qd_hbm, wqd), ("q_gain", query_gain_hbm, query_gain_ref),
+        ("nope", nope_hbm, wnope), ("rup", rupt_hbm, wrup), ("kup", kup_hbm, wkup), ("init_c", init_c_hbm, init_c_ref),
+        ("init_n", init_n_hbm, init_n_ref), ("h_gain", head_gain_hbm, head_gain_ref), ("vup", vup_hbm, wvup),
+        ("oa", oa_hbm, wout.at[0:128]), ("or", or_hbm, wout.at[128:256]),
+    )
+    loads = {name: pltpu.make_async_copy(src, dst, wsem.at[i]) for i, (name, src, dst) in enumerate(plan)}
+    for c in loads.values():
+        c.start()
+
+    def ready(*names):
+        for name in names:
+            loads[name].wait()
+
     barrier = pltpu.get_barrier_semaphore()
     peers = 0
     for d in range(1, NY):
@@ -108,22 +127,11 @@
         pl.semaphore_signal(barrier, inc=1, device_id={"x": g // NC, "c": lax.rem(g, NC)}, device_id_type=MESH_ID)
         peers += 1
 
-    loads = [
-        pltpu.make_async_copy(src, dst, wsem.at[i])
-        for i, (src, dst) in enumerate(
-            [
-                (kvd_hbm, wkv), (ropet_hbm, wrope), (rk_hbm, wt.at[0:MK]), (rq_hbm, wt.at[MK : 2 * MK]), (rv_hbm, wv),
-                (qd_hbm, wqd), (nope_hbm, wnope), (rupt_hbm, wrup), (kup_hbm, wkup), (vup_hbm, wvup),
-                (oa_hbm, wout.at[0:128]), (or_hbm, wout.at[128:256]),
-            ]
-        )
-    ]
-    for c in loads:
-        c.start()
-
+    ready("rows", "in_gain")
     normed = rms(rows_ref[...].astype(F32), in_gain_ref[...]).astype(BF16)
     own_rows = pl.ds(pl.multiple_of(yi * R, R), R)
     nb[own_rows, :] = normed
+    ready("gates")
     wt[2 * MK : 2 * MK + 16, :] = jnp.concatenate(
         [gates_ref[...], jnp.zeros((12, gates_ref.shape[1]), BF16)], axis=0
     )
@@ -137,6 +145,7 @@
         c.start()
 
     sp_index = (zi * NX + xi) * NC + ci
+    ready("kv", "rope", "kv_gain", "blocks", "table")
     block_row = block_tab_ref[pl.ds(sp_index, 1), :]
     cos_b, sin_b = block_row[:, :ROPE], block_row[:, ROPE:]
 
@@ -144,8 +153,6 @@
         cos_r, sin_r = table[:, :ROPE], table[:, ROPE:]
         return cos_b * cos_r - sin_b * sin_r, sin_b * cos_r + cos_b * sin_r
 
-    loads[0].wait()
-    loads[1].wait()
     latent = rms(nn(normed, wkv[...]), kv_gain_ref[...]).astype(BF16)
     rope = rotated(nt(normed, wrope[...]), *angles(row_tab_ref[own_rows, :])).astype(BF16)
     own_chunk = pl.ds(pl.multiple_of(zi * H, H), H)
@@ -163,8 +170,7 @@
 
     lax.fori_loop(1, NZ, start_z_key, 0)
 
-    for i in (2, 3, 4, 5):
-        loads[i].wait()
+    ready("rk", "rq", "rv", "forget")
     for d in range(1, NY):
         rows = pl.ds(pl.multiple_of(lax.rem(yi - d + NY, NY) * R, R), R)
         to_y(d, nb.at[rows], nb.at[rows], ny_s, ny_r).wait_recv()
@@ -213,8 +219,7 @@
         c.start()
     ra[me] = sa[me]
 
-    for i in (6, 7, 8):
-        loads[i].wait()
+    ready("qd", "q_gain", "nope", "rup", "kup")
     q_latent = rms(nn(nb[...], wqd[...]), query_gain_ref[...]).astype(BF16)
     q_nope = nn(q_latent, wnope[...]).astype(BF16)
     q_abs = nt(q_nope, wkup[...]).astype(BF16)
@@ -341,6 +346,7 @@
         return 0
 
     lax.fori_loop(1, NZ, wait_z_total, 0)
+    ready("init_c", "init_n", "h_gain")
     own_slice = pl.ds(pl.multiple_of(me * SR, SR), SR)
     pad = jnp.zeros((1, 128 - MK), F32)
 
@@ -417,8 +423,7 @@
     mass = functools.reduce(jnp.add, parts)
     merged = functools.reduce(jnp.add, [p * rp[h].astype(F32) for h, p in enumerate(parts)])
     attended = (merged / mass).astype(BF16)
-    for i in (9, 10, 11):
-        loads[i].wait()
+    ready("vup", "oa", "or")
     attention = nn(attended, wvup[...]).astype(BF16)
     joined = jnp.concatenate([attention, recurrent], axis=1)
     ob[...] = nn(joined, wout[...]).astype(BF16)
@@ -471,7 +476,7 @@
     H = R // 2
     KEYS = NZ * H
     block_tab, row_tab = rotary_tables(NZ * G, T)
-    vmem_args = (
+    small_args = (
         rows_in, in_gain.reshape(1, -1), query_gain.reshape(1, -1), kv_gain.reshape(1, -1), gate_weight[:, :, 0].T,
         forget_level[:, :, 0].T, head_gain.reshape(1, -1), init_state[:, 0], init_norm[:, 0],
         jnp.asarray(block_tab), jnp.asarray(row_tab),
@@ -484,11 +489,10 @@
     return pl.pallas_call(
         functools.partial(body, sizes),
         out_shape=jax.ShapeDtypeStruct((R, D), BF16),
-        in_specs=[pl.BlockSpec(memory_space=pltpu.VMEM)] * len(vmem_args)
-        + [pl.BlockSpec(memory_space=pltpu.HBM)] * len(hbm_args),
+        in_specs=[pl.BlockSpec(memory_space=pltpu.HBM)] * (len(small_args) + len(hbm_args)),
         out_specs=pl.BlockSpec(memory_space=pltpu.VMEM),
         scratch_shapes=[
-            *[pltpu.VMEM(a.shape, BF16) for a in hbm_args[:7]],
+            *[pltpu.VMEM(a.shape, a.dtype) for a in (*small_args, *hbm_args[:7])],
             pltpu.VMEM((2 * MK + 16, D), BF16),
             pltpu.VMEM(rec_value.shape, BF16),
             pltpu.VMEM((256, D), BF16),
@@ -515,7 +519,7 @@
             pltpu.VMEM((NY, 8, T), F32),
             pltpu.VMEM((T, D), BF16),
             pltpu.VMEM((NY, R, D), BF16),
-            dma((12,)),
+            dma((23,)),
             *[dma((NY,))] * 2,
             *[dma((NZ,))] * 2,
             *[dma((NX,))] * 4,
@@ -525,10 +529,10 @@
             *[dma((NY,))] * 8,
         ],
         compiler_params=pltpu.CompilerParams(
-            collective_id=0, has_side_effects=True, vmem_limit_bytes=48 * 1024 * 1024
+            collective_id=0, has_side_effects=True, vmem_limit_bytes=62 * 1024 * 1024
         ),
         name="layer",
-    )(*vmem_args, *hbm_args)
+    )(*small_args, *hbm_args)
 
 
 def solution(mesh):

time: 74.3 us -> 59 us (0.79)
  the two profiles are of different devices: /device:TPU:32 before, /device:TPU:1 now
where the time goes in v2:
time: 59 us; the launch traced here: 57.9 us
  Pallas kernels  56.4 us (96%)
  local copies, waits for them, and re-layouts  1.57 us (3%)
    pallas_call x1, Pallas kernels, shards(): pl.pallas_call(functools.partial(body, sizes), out_shape=jax.ShapeDtypeSt...  56.4 us
    unnamed x1, local copies, waits for them, and re-layouts  1.57 us

profile of v2, /device:TPU:1, one launch (start us, length us, event | category | flops | bytes accessed | tf_op | source)
XLA Modules:
  0.0 57.9 jit_solution(16853772928473723663)
XLA Ops:
  0.0 56.4 %layer.1 = bf16[32,2048]{1,0:T(8,128)(2,1)} custom-call(bf16[32,2048]{1,0:T(8,128)(2,1)} %rows_hbm.1, f32[1,2048]{1,0:T(1,128)} %bitcast.22, f32[1,256]{1,0:T(1,128)} %bitcast.23, f32[1,128]{1,0:T(1,128)} %bitcast.26, bf16[4,2048]{1,0:T(4,128)(2,1)} %bitcast.21, f32[2,128]{1,0:T(2,128)} %bitcast.24, f32[1,128]{1,0:T(1,128)} %bitcast.27, ...), custom_call_target="tpu_custom_call" | custom-call | tf_op jit(solution)/shard_map/layer/pallas_call | solution.py:489
  56.4 1.6 %copy.25 = bf16[32,2048]{1,0:T(8,128)(2,1)} copy(bf16[32,2048]{1,0:T(8,128)(2,1)} %layer.1) | data formatting | bytes 262144
